TPU v7x, 32 devices: a whole 2x2x4 slice. The times are simulated.
32 devices in a mesh: sp: 8 (over z, y), tp: 4 (over x, core).
Axes of the slice: x: 2, y: 2, z: 4, core: 2. Of those that a mesh axis runs over, the one named last changes fastest.
Arguments:
- resid_in: bfloat16 [3072, 2048], P('sp'), may hold values from -6 to 6
- cotangent: bfloat16 [3072, 2048], P('sp'), may hold values from -2 to 2
- norm_gain: float32 [2048], replicated, may hold values from 0.1 to 1.9
- routes: int32 [3072, 2], P('sp'), may hold values from 0 to 7, all different within a row; in each aligned block of 384 rows (0 to 383, 384 to 767, ...) at most 192 rows name the same one
- route_weights: float32 [3072, 2], P('sp'), may hold values from 0.1 to 1
- gate_weight: bfloat16 [8, 2048, 1024], P('sp', None, 'tp'), may hold values from -0.125 to 0.125
- up_weight: bfloat16 [8, 2048, 1024], P('sp', None, 'tp'), may hold values from -0.125 to 0.125
- down_weight: bfloat16 [8, 1024, 2048], P('sp', 'tp'), may hold values from -0.1875 to 0.1875
- out_weight: bfloat16 [2048, 1024], P(None, 'tp'), may hold values from -0.1875 to 0.1875
- gate_b: bfloat16 [3072, 1024], P('sp', 'tp'), may hold values from -6 to 6
- gate_c: bfloat16 [3072, 1024], P('sp', 'tp'), may hold values from -6 to 6
- values_u: bfloat16 [3072, 1024], P('sp', 'tp'), may hold values from -6 to 6
- taps: float32 [3, 1024], P(None, 'tp'), may hold values from -3.5 to 3.5
Outputs:
- grad_gate_weight: float32 [8, 2048, 1024], P('sp', None, 'tp')
- grad_up_weight: float32 [8, 2048, 1024], P('sp', None, 'tp')
- grad_down_weight: float32 [8, 1024, 2048], P('sp', 'tp')
- grad_resid: bfloat16 [3072, 2048], P('sp')
- grad_out_weight: float32 [2048, 1024], P('sp', 'tp')
- grad_gate_b: bfloat16 [3072, 1024], P('sp', 'tp')
- grad_gate_c: bfloat16 [3072, 1024], P('sp', 'tp')
- grad_values: bfloat16 [3072, 1024], P('sp', 'tp')
Inputs may be any that keep to these rules, and one draw needn't show every extreme that they name: `routes`: A row's 2 experts differ. In the rows of one index of sp (384 tokens) no expert is named more than 192 times, a bound that some block reaches.
All inputs are finite; a program needn't handle non-finite values.
Results may differ from a plain program's by a relative error of at most 0.024.
Values may be sent and summed in bfloat16 or wider, within the bound.
A program may use at most 128 MiB of HBM per device.

v0:
```python
import jax
import jax.numpy as jnp
from jax import lax
from jax.sharding import PartitionSpec as P

norm_eps = 1e-06


def passed_along(array, axis, by):
    size = lax.axis_size(axis)
    pairs = [(i, i + by) for i in range(size) if 0 <= i + by < size]
    return lax.ppermute(array, axis, pairs)


def expert_pass(entry_rows, entry_cots, entry_weights, gate_mat, up_mat, down_mat):
    f32 = jnp.float32
    bf16 = jnp.bfloat16
    gate_pre = jnp.dot(entry_rows, gate_mat, preferred_element_type=f32)
    up_pre = jnp.dot(entry_rows, up_mat, preferred_element_type=f32)
    logistic = jax.nn.sigmoid(gate_pre)
    activated = gate_pre * logistic
    hidden = (activated * up_pre * entry_weights[:, None]).astype(bf16)
    grad_down = jnp.einsum("rf,rd->fd", hidden, entry_cots, preferred_element_type=f32)
    dhidden = (
        jnp.einsum("rd,fd->rf", entry_cots, down_mat, preferred_element_type=f32)
        * entry_weights[:, None]
    )
    dgate = (dhidden * up_pre * logistic * (1.0 + gate_pre * (1.0 - logistic))).astype(bf16)
    dup = (dhidden * activated).astype(bf16)
    grad_gate = jnp.einsum("rd,rf->df", entry_rows, dgate, preferred_element_type=f32)
    grad_up = jnp.einsum("rd,rf->df", entry_rows, dup, preferred_element_type=f32)
    partial_sum = jnp.einsum("rf,df->rd", dgate, gate_mat, preferred_element_type=f32) + jnp.einsum(
        "rf,df->rd", dup, up_mat, preferred_element_type=f32
    )
    return (grad_gate, grad_up, grad_down, partial_sum)


def on_device(
    resid_in,
    cotangent,
    norm_gain,
    routes,
    route_weights,
    gate_weight,
    up_weight,
    down_weight,
    out_weight,
    gate_b,
    gate_c,
    values_u,
    taps,
):
    f32 = jnp.float32
    bf16 = jnp.bfloat16
    token_count, model_width = resid_in.shape
    groups = lax.axis_size("sp")
    lanes = lax.axis_size("tp")
    local_experts = gate_weight.shape[0]
    expert_total = local_experts * groups
    capacity = 4 * token_count // expert_total
    slot_span = local_experts * capacity
    resid_wide = resid_in.astype(f32)
    inv_rms = lax.rsqrt(jnp.mean(resid_wide * resid_wide, axis=1, keepdims=True) + norm_eps)
    normed = (resid_wide * inv_rms * norm_gain).astype(bf16)
    mixed = gate_c.astype(f32) * values_u.astype(f32)
    earlier = passed_along(mixed[-2:], "sp", 1)
    quarter = model_width // lanes
    lane = lax.axis_index("tp")
    slots = expert_total * capacity
    names = jnp.arange(expert_total, dtype=jnp.int32)
    chosen = routes[:, :, None] == names[None, None, :]
    named = jnp.any(chosen, axis=1).astype(bf16)
    order = jnp.arange(token_count, dtype=jnp.int32)
    strict = (order[:, None] > order[None, :]).astype(bf16)
    before = jnp.dot(strict, named, preferred_element_type=f32).astype(jnp.int32)
    rank = jnp.sum(jnp.where(chosen, before[:, None, :], 0), axis=2)
    targets = routes * capacity + rank
    slot_ids = jnp.arange(slots, dtype=jnp.int32)[:, None]
    first = slot_ids == targets[:, 0][None, :]
    second = slot_ids == targets[:, 1][None, :]
    placing = (first | second).astype(bf16)
    sent_weights = jnp.sum(
        jnp.where(first, route_weights[:, 0][None, :], 0.0)
        + jnp.where(second, route_weights[:, 1][None, :], 0.0),
        axis=1,
    ).reshape(groups, slot_span)
    own_rows = lax.dynamic_slice_in_dim(normed, lane * quarter, quarter, axis=1)
    own_cots = lax.dynamic_slice_in_dim(cotangent, lane * quarter, quarter, axis=1)
    sent_rows = jnp.dot(placing, own_rows, preferred_element_type=f32).astype(bf16)
    sent_cots = jnp.dot(placing, own_cots, preferred_element_type=f32).astype(bf16)
    sent_rows = sent_rows.reshape(groups, slot_span, quarter)
    sent_cots = sent_cots.reshape(groups, slot_span, quarter)
    got_weights = lax.all_to_all(sent_weights, "sp", split_axis=0, concat_axis=0, tiled=True)
    got_rows = lax.all_gather(
        lax.all_to_all(sent_rows, "sp", split_axis=0, concat_axis=0, tiled=True),
        "tp",
        axis=2,
        tiled=True,
    )
    got_cots = lax.all_gather(
        lax.all_to_all(sent_cots, "sp", split_axis=0, concat_axis=0, tiled=True),
        "tp",
        axis=2,
        tiled=True,
    )
    grads_gate, grads_up, grads_down, terms = ([], [], [], [])
    entry_rows = got_rows.reshape(groups * capacity, model_width)
    entry_cots = got_cots.reshape(groups * capacity, model_width)
    entry_weights = got_weights.reshape(groups * capacity)
    grad_gate, grad_up, grad_down, partial_sum = expert_pass(
        entry_rows, entry_cots, entry_weights, gate_weight[0], up_weight[0], down_weight[0]
    )
    grads_gate.append(grad_gate)
    grads_up.append(grad_up)
    grads_down.append(grad_down)
    terms.append(partial_sum.astype(bf16).reshape(groups, capacity, model_width))
    expert_term = terms[0]
    summed = (
        lax.psum_scatter(expert_term, "tp", scatter_dimension=2, tiled=True)
        .astype(jnp.float32)
        .astype(bf16)
    )
    returned = lax.all_to_all(summed, "sp", split_axis=0, concat_axis=0, tiled=True).reshape(
        expert_total * capacity, model_width // lanes
    )
    own_grad = jnp.einsum("st,sq->tq", placing, returned, preferred_element_type=f32)
    dnormed = lax.all_gather(own_grad.astype(bf16), "tp", axis=1, tiled=True).astype(f32)
    scaled = dnormed * norm_gain
    resid_grad = (
        cotangent.astype(f32)
        + inv_rms * scaled
        - resid_wide * inv_rms**3 * jnp.mean(scaled * resid_wide, axis=1, keepdims=True)
    )
    grad_resid = resid_grad.astype(bf16)
    extended = jnp.concatenate([earlier, mixed], axis=0)
    conv = (
        taps[0] * extended[:token_count]
        + taps[1] * extended[1 : token_count + 1]
        + taps[2] * extended[2 : token_count + 2]
    )
    merged = (gate_b.astype(f32) * conv).astype(bf16)
    grad_out_weight = lax.psum_scatter(
        jnp.einsum("td,tc->dc", grad_resid, merged, preferred_element_type=f32).astype(
            jnp.bfloat16
        ),
        "sp",
        scatter_dimension=0,
        tiled=True,
    ).astype(jnp.float32)
    dmerged = jnp.dot(grad_resid, out_weight, preferred_element_type=f32)
    grad_gate_b = (dmerged * conv).astype(bf16)
    dconv = dmerged * gate_b.astype(f32)
    later = passed_along(dconv[:2], "sp", -1)
    extended_grad = jnp.concatenate([dconv, later], axis=0)
    dmixed = (
        taps[2] * extended_grad[:token_count]
        + taps[1] * extended_grad[1 : token_count + 1]
        + taps[0] * extended_grad[2 : token_count + 2]
    )
    grad_gate_c = (dmixed * values_u.astype(f32)).astype(bf16)
    grad_values = (dmixed * gate_c.astype(f32)).astype(bf16)
    return (
        jnp.stack(grads_gate),
        jnp.stack(grads_up),
        jnp.stack(grads_down),
        grad_resid,
        grad_out_weight,
        grad_gate_b,
        grad_gate_c,
        grad_values,
    )


def solution(mesh):
    placed = (
        P("sp", None),
        P("sp", None),
        P(),
        P("sp", None),
        P("sp", None),
        P("sp", None, "tp"),
        P("sp", None, "tp"),
        P("sp", "tp", None),
        P(None, "tp"),
        P("sp", "tp"),
        P("sp", "tp"),
        P("sp", "tp"),
        P(None, "tp"),
    )
    return jax.shard_map(
        on_device,
        mesh=mesh,
        in_specs=placed,
        out_specs=(
            P("sp", None, "tp"),
            P("sp", None, "tp"),
            P("sp", "tp", None),
            P("sp", None),
            P("sp", "tp"),
            P("sp", "tp"),
            P("sp", "tp"),
            P("sp", "tp"),
        ),
        check_vma=False,
    )
```

profile of v0, /device:TPU:0, one launch (start us, length us, event | category | flops | bytes accessed | tf_op | source)
XLA Modules:
  0.0 364.5 jit_solution(5835447940842580865)
XLA Ops:
  7.2 0.0 copy-start
  7.2 0.0 all-gather.4.cloned.1.call-start
  7.3 3.6 convert_element_type.75
  10.8 0.4 multiply_reduce_fusion.1
  11.2 0.1 convolution_convert_fusion.3
  11.4 0.1 select_reduce_fusion
  11.5 0.1 dynamic-slice
  11.6 2.2 convolution_convert_fusion.1
  13.8 44.2 %all_to_all.24 = bf16[8,192,512]{2,1,0:T(8,128)(2,1)} all-to-all(bf16[8,192,512]{2,1,0:T(8,128)(2,1)S(1)} %bitcast.47), channel_id=1, replica_groups=mesh['sp'=8,'tp'=4] {'sp'}, dimensions={0} | all-to-all | bytes 3145728 | tf_op jit(solution)/shard_map/all_to_all | solution.py:95
  58.0 0.0 all-gather.4.cloned.1.call-update
  58.0 0.0 all-gather.6.cloned.1.call-start
  58.1 2.0 convolution_convert_fusion
  60.1 40.2 %all_to_all.25 = bf16[8,192,512]{2,1,0:T(8,128)(2,1)} all-to-all(bf16[8,192,512]{2,1,0:T(8,128)(2,1)S(1)} %bitcast.48), channel_id=1, replica_groups=mesh['sp'=8,'tp'=4] {'sp'}, dimensions={0} | all-to-all | bytes 3145728 | tf_op jit(solution)/shard_map/all_to_all | solution.py:101
  100.3 0.0 all-gather.6.cloned.1.call-update
  100.3 0.0 reduce-scatter.3.cloned.1.call-start
  100.4 0.6 add_reduce_fusion
  101.0 0.1 all_to_all.17
  101.0 9.9 %all_to_all.26 = f32[8,1,192]{2,1,0:T(1,128)S(1)} all-to-all(f32[8,1,192]{2,1,0:T(1,128)S(1)} %all_to_all.17), channel_id=1, replica_groups=mesh['sp'=8,'tp'=4] {'sp'}, dimensions={0} | all-to-all | bytes 12288 | tf_op jit(solution)/shard_map/all_to_all | solution.py:93
  110.9 0.1 mul.171
  111.0 6.7 %fusion.17 = f32[1536,256]{1,0:T(8,128)} fusion(bf16[1536,2048]{1,0:T(8,128)(2,1)} %bitcast.55, bf16[1,2048,256]{2,1,0:T(8,128)(2,1)S(1)} %copy-done), kind=kOutput, calls=%fused_computation.32 | convolution fusion | flops 1610612736 | bytes 8912896 | tf_op jit(solution)/shard_map/dot_general | solution.py:18
  117.7 0.5 copy-done.17
  118.2 3.0 fusion.20
  121.2 30.3 %all-gather.6.cloned.1.call-done = bf16[8,192,2048]{2,1,0:T(8,128)(2,1)} async-done(((bf16[8,192,512]{2,1,0:T(8,128)(2,1)}), bf16[8,192,2048]{2,1,0:T(8,128)(2,1)}) %all-gather.6.cloned.1.call-update) | async-done | bytes 6291472 | tf_op jit(solution)/shard_map/all_gather | solution.py:100
  151.5 6.4 %multiply_convert_fusion.1 = (bf16[1536,256]{1,0:T(8,128)(2,1)S(1)}, bf16[1536,256]{1,0:T(8,128)(2,1)S(1)}) fusion(f32[1536,256]{1,0:T(8,128)} %fusion.17, f32[1536,256]{1,0:T(8,128)} %fusion.20, f32[1536]{0:T(1024)S(1)} %mul.171, bf16[1536,2048]{1,0:T(8,128)(2,1)} %bitcast.59, bf16[1,256,2048]{2,1,0:T(8,128)(2,1)} %param.20), kind=kOutput, calls=%fused_computation.17 | convolution fusion | flops 1616117760 | bytes 12064768 | tf_op jit(solution)/shard_map/rd,fd->rf/dot_general | solution.py:25
  158.0 1.8 fusion.15
  159.8 4.4 %add_convert_fusion = bf16[1536,2048]{1,0:T(8,128)(2,1)} fusion(f32[1536,2048]{1,0:T(8,128)S(1)} %fusion.15, bf16[1536,256]{1,0:T(8,128)(2,1)S(1)} %get-tuple-element.16, bf16[1,2048,256]{2,1,0:T(8,128)(2,1)S(1)} %copy-done.6), kind=kOutput, calls=%fused_computation | convolution fusion | flops 1616904192 | bytes 20709376 | tf_op jit(solution)/shard_map/rf,df->rd/dot_general | solution.py:32
  164.3 0.0 reduce-scatter.3.cloned.1.call-update
  164.3 0.0 all-gather.8.cloned.1.call-start
  164.3 58.0 %reduce-scatter.3.cloned.1.call-done = bf16[8,192,512]{2,1,0:T(8,128)(2,1)} async-done(((bf16[8,192,2048]{2,1,0:T(8,128)(2,1)}), bf16[8,192,512]{2,1,0:T(8,128)(2,1)}) %reduce-scatter.3.cloned.1.call-update) | async-done | bytes 1572880 | tf_op jit(solution)/shard_map/reduce_scatter | solution.py:119
  222.3 42.4 %all_to_all.27 = bf16[8,192,512]{2,1,0:T(8,128)(2,1)S(1)} all-to-all(bf16[8,192,512]{2,1,0:T(8,128)(2,1)} %reduce-scatter.3.cloned.1.call-done), channel_id=1, replica_groups=mesh['sp'=8,'tp'=4] {'sp'}, dimensions={0} | all-to-all | bytes 3145728 | tf_op jit(solution)/shard_map/all_to_all | solution.py:123
  264.7 1.6 fusion.6
  266.3 0.0 all-gather.8.cloned.1.call-update
  266.3 0.0 reduce-scatter.5.cloned.1.call-start
  266.4 3.6 collective-permute-start
  270.0 14.1 %all-gather.8.cloned.1.call-done = bf16[384,2048]{1,0:T(8,128)(2,1)} async-done(((bf16[384,512]{1,0:T(8,128)(2,1)}), bf16[384,2048]{1,0:T(8,128)(2,1)}) %all-gather.8.cloned.1.call-update) | async-done | bytes 1572880 | tf_op jit(solution)/shard_map/all_gather | solution.py:127
  284.1 2.1 multiply_reduce_fusion
  286.3 2.5 subtract_convert_fusion
  288.9 1.3 multiply_convert_fusion.4
  290.2 1.8 convolution_convert_fusion.2
  292.0 0.0 reduce-scatter.5.cloned.1.call-update
  292.0 6.2 %convolution_bitcast_fusion.2 = f32[1,2048,256]{2,1,0:T(8,128)} fusion(bf16[1536,2048]{1,0:T(8,128)(2,1)} %bitcast.56, bf16[1536,256]{1,0:T(8,128)(2,1)S(1)} %get-tuple-element.17), kind=kOutput, calls=%fused_computation.10 | convolution fusion | flops 1610612736 | bytes 9175040 | tf_op jit(solution)/shard_map/rd,rf->df/dot_general | solution.py:30
  298.2 6.3 %convolution_bitcast_fusion = f32[1,256,2048]{2,1,0:T(8,128)} fusion(bf16[1536,2048]{1,0:T(8,128)(2,1)} %bitcast.60, f32[1536,256]{1,0:T(8,128)S(1)} %copy-done.21, f32[1536]{0:T(1024)S(1)} %mul.171, f32[1536,256]{1,0:T(8,128)S(1)} %copy-done.20), kind=kOutput, calls=%fused_computation.8 | convolution fusion | flops 1613365248 | bytes 11540480 | tf_op jit(solution)/shard_map/rf,rd->fd/dot_general | solution.py:23
  304.5 1.4 collective-permute-start.1
  305.9 6.1 %convolution_bitcast_fusion.1 = f32[1,2048,256]{2,1,0:T(8,128)} fusion(bf16[1536,2048]{1,0:T(8,128)(2,1)} %bitcast.57, bf16[1536,256]{1,0:T(8,128)(2,1)S(1)} %copy-done.8), kind=kOutput, calls=%fused_computation.9 | convolution fusion | flops 1610612736 | bytes 9175040 | tf_op jit(solution)/shard_map/rd,rf->df/dot_general | solution.py:31
  312.0 0.8 fusion.35
  312.9 0.7 fusion.36
  313.6 42.8 %reduce-scatter.5.cloned.1.call-done = bf16[256,256]{1,0:T(8,128)(2,1)} async-done(((bf16[2048,256]{1,0:T(8,128)(2,1)}), bf16[256,256]{1,0:T(8,128)(2,1)}) %reduce-scatter.5.cloned.1.call-update) | async-done | bytes 131088 | tf_op jit(solution)/shard_map/reduce_scatter | solution.py:142
  356.3 1.6 convert_element_type.92
  (56 shorter events, 0.3 us)
Async XLA Ops:
  7.2 103.8 %copy-start = (bf16[1,2048,256]{2,1,0:T(8,128)(2,1)S(1)}, bf16[1,2048,256]{2,1,0:T(8,128)(2,1)}, u32[]{:S(2)}) copy-start(bf16[1,2048,256]{2,1,0:T(8,128)(2,1)} %param.18) | copy-start | bytes 3145732
  7.2 103.8 %all-gather.4.cloned.1.call-start = ((), (), s32[]{:S(2)}) async-start(), calls=%async_computation.6 | async-start | bytes 7864320 | tf_op jit(solution)/shard_map/all_gather | solution.py:94
  7.2 3.6 copy-start.2
  7.2 4.0 %copy-start.14 = (s32[384,2]{0,1:T(2,128)S(1)}, s32[384,2]{0,1:T(2,128)}, u32[]{:S(2)}) copy-start(s32[384,2]{0,1:T(2,128)} %param.16) | copy-start | bytes 9220
  7.3 4.3 %copy-start.13 = (f32[2048]{0:T(1024)S(1)}, f32[2048]{0:T(1024)}, u32[]{:S(2)}) copy-start(f32[2048]{0:T(1024)} %param.15) | copy-start | bytes 24580
  58.0 93.5 %all-gather.6.cloned.1.call-start = ((), (), s32[]{:S(2)}) async-start(), calls=%async_computation.7 | async-start | bytes 7864320 | tf_op jit(solution)/shard_map/all_gather | solution.py:100
  60.1 40.3 %copy-start.15 = (f32[384,2]{0,1:T(2,128)S(1)}, f32[384,2]{0,1:T(2,128)}, u32[]{:S(2)}) copy-start(f32[384,2]{0,1:T(2,128)} %param.17) | copy-start | bytes 9220
  100.3 122.0 %reduce-scatter.3.cloned.1.call-start = ((), (), s32[]{:S(2)}) async-start(), calls=%async_computation.8 | async-start | bytes 7864320 | tf_op jit(solution)/shard_map/reduce_scatter | solution.py:119
  111.0 6.7 %copy-start.5 = (bf16[1,2048,256]{2,1,0:T(8,128)(2,1)S(1)}, bf16[1,2048,256]{2,1,0:T(8,128)(2,1)}, u32[]{:S(2)}) copy-start(bf16[1,2048,256]{2,1,0:T(8,128)(2,1)} %param.19) | copy-start | bytes 3145732
  111.0 7.2 %copy-start.17 = (bf16[8,192,2048]{2,1,0:T(8,128)(2,1)S(1)}, bf16[8,192,2048]{2,1,0:T(8,128)(2,1)}, u32[]{:S(2)}) copy-start(bf16[8,192,2048]{2,1,0:T(8,128)(2,1)} %all-gather.4.cloned.1.call-done) | copy-start | bytes 18874372
  158.0 1.9 copy-start.7
  158.0 1.9 copy-start.6
  164.3 119.9 %all-gather.8.cloned.1.call-start = ((), (), s32[]{:S(2)}) async-start(), calls=%async_computation.9 | async-start | bytes 1966080 | tf_op jit(solution)/shard_map/all_gather | solution.py:127
  264.7 1.7 copy-start.9
  264.7 1.7 copy-start.11
  264.7 5.3 %copy-start.16 = (f32[3,256]{1,0:T(4,128)S(1)}, f32[3,256]{1,0:T(4,128)}, u32[]{:S(2)}) copy-start(f32[3,256]{1,0:T(4,128)} %param.25) | copy-start | bytes 9220
  266.3 90.0 %reduce-scatter.5.cloned.1.call-start = ((), (), s32[]{:S(2)}) async-start(), calls=%async_computation.10 | async-start | bytes 1179648 | tf_op jit(solution)/shard_map/reduce_scatter | solution.py:142
  266.4 22.4 %collective-permute-start = (f32[2,256]{1,0:T(2,128)S(1)}, f32[2,256]{1,0:T(2,128)S(1)}, u32[]{:S(2)}, u32[]{:S(2)}) collective-permute-start(f32[2,256]{1,0:T(2,128)S(1)} %slice.57), channel_id=1, source_target_pairs={{0,4},{4,8},{8,12},{12,16},{16,20},{20,24},{24,28},{1,5},{5,9},{9,... | collective-permute-start | bytes 6152 | tf_op jit(solution)/shard_map/ppermute | solution.py:12
  284.1 2.1 copy-start.3
  286.3 2.6 copy-start.18
  286.3 2.6 copy-start.19
  288.8 1.3 copy-start.4
  292.0 6.2 %copy-start.20 = (f32[1536,256]{1,0:T(8,128)S(1)}, f32[1536,256]{1,0:T(8,128)}, u32[]{:S(2)}) copy-start(f32[1536,256]{1,0:T(8,128)} %fusion.17) | copy-start | bytes 4718596
  292.0 6.2 %copy-start.21 = (f32[1536,256]{1,0:T(8,128)S(1)}, f32[1536,256]{1,0:T(8,128)}, u32[]{:S(2)}) copy-start(f32[1536,256]{1,0:T(8,128)} %fusion.20) | copy-start | bytes 4718596
  298.2 7.7 %copy-start.8 = (bf16[1536,256]{1,0:T(8,128)(2,1)S(1)}, bf16[1536,256]{1,0:T(8,128)(2,1)}, u32[]{:S(2)}) copy-start(bf16[1536,256]{1,0:T(8,128)(2,1)} %copy-done.7) | copy-start | bytes 2359300
  304.5 7.6 %copy-start.12 = (bf16[384,256]{1,0:T(8,128)(2,1)S(1)}, bf16[384,256]{1,0:T(8,128)(2,1)}, u32[]{:S(2)}) copy-start(bf16[384,256]{1,0:T(8,128)(2,1)} %param.23) | copy-start | bytes 589828
  304.5 8.4 %copy-start.10 = (bf16[384,256]{1,0:T(8,128)(2,1)S(1)}, bf16[384,256]{1,0:T(8,128)(2,1)}, u32[]{:S(2)}) copy-start(bf16[384,256]{1,0:T(8,128)(2,1)} %param.24) | copy-start | bytes 589828
  304.5 7.6 %collective-permute-start.1 = (f32[2,256]{1,0:T(2,128)S(1)}, f32[2,256]{1,0:T(2,128)S(1)}, u32[]{:S(2)}, u32[]{:S(2)}) collective-permute-start(f32[2,256]{1,0:T(2,128)S(1)} %slice.60), channel_id=1, source_target_pairs={{4,0},{8,4},{12,8},{16,12},{20,16},{24,20},{28,24},{5,1},{9,5},{13... | collective-permute-start | bytes 6152 | tf_op jit(solution)/shard_map/ppermute | solution.py:12
  305.9 52.1 %copy-start.1 = (bf16[1,2048,256]{2,1,0:T(8,128)(2,1)S(1)}, bf16[1,2048,256]{2,1,0:T(8,128)(2,1)}, u32[]{:S(2)}) copy-start(bf16[1,2048,256]{2,1,0:T(8,128)(2,1)} %param.18) | copy-start | bytes 3145732
Sparse Core Ops, SparseCore 0:
  58.2 45.3 all-gather.3
  105.1 46.3 all-gather.5
  164.4 57.8 reduce-scatter.2
  266.4 17.6 all-gather.7
  292.1 64.1 reduce-scatter.4
where the time goes:
time: 365 us; the launch traced here: 364 us
  waiting for transfers between devices  145 us (40%)
  blocking collectives  137 us (38%)
  matrix products  49.9 us (14%)
  between operations  14.1 us (4%)
  other arithmetic  12.5 us (3%)
  starting transfers between devices  5.21 us (1%)
    reduce_scatter x1, waiting for transfers between devices, on_device(): lax.psum_scatter(expert_term, 'tp', scatter_dimension=2, tiled=True)  58 us
    all_to_all x1, blocking collectives, on_device(): lax.all_to_all(sent_rows, 'sp', split_axis=0, concat_axis=0, tiled=True)  44.2 us
    reduce_scatter x1, waiting for transfers between devices, on_device(): lax.psum_scatter(jnp.einsum('td,tc->dc', grad_resid, merged, preferred_el...  42.8 us
    all_to_all x1, blocking collectives, on_device(): lax.all_to_all(summed, 'sp', split_axis=0, concat_axis=0, tiled=True)  42.4 us
    all_to_all x1, blocking collectives, on_device(): lax.all_to_all(sent_cots, 'sp', split_axis=0, concat_axis=0, tiled=True)  40.2 us
    all_gather x1, waiting for transfers between devices, on_device(): lax.all_gather(lax.all_to_all(sent_cots, 'sp', split_axis=0, concat_axis=...  30.3 us
    all_gather x1, waiting for transfers between devices, on_device(): lax.all_gather(own_grad.astype(bf16), 'tp', axis=1, tiled=True).astype(f32)  14.1 us
    all_to_all x1, blocking collectives, on_device(): lax.all_to_all(sent_weights, 'sp', split_axis=0, concat_axis=0, tiled=True)  9.85 us
  transfers between devices with their start and end apart: 7, of which 4 were waited for; matrix products, arithmetic and copies ran while one was open for 10% of the time, Pallas kernels for 0%

commit v1 on v0

--- a/solution.py
+++ b/solution.py
@@ -50,6 +50,11 @@
     values_u,
     taps,
 ):
+
+    def store_the_levels_all(slab_in, dim_no=2):
+        all_values = lax.all_gather(slab_in, axis_name="tp")
+        return jnp.concatenate(all_values, dim_no)
+
     f32 = jnp.float32
     bf16 = jnp.bfloat16
     token_count, model_width = resid_in.shape
@@ -97,11 +102,8 @@
         axis=2,
         tiled=True,
     )
-    got_cots = lax.all_gather(
-        lax.all_to_all(sent_cots, "sp", split_axis=0, concat_axis=0, tiled=True),
-        "tp",
-        axis=2,
-        tiled=True,
+    got_cots = store_the_levels_all(
+        lax.all_to_all(sent_cots, "sp", split_axis=0, concat_axis=0, tiled=True)
     )
     grads_gate, grads_up, grads_down, terms = ([], [], [], [])
     entry_rows = got_rows.reshape(groups * capacity, model_width)

time: 365 us -> 377 us (1.033)
  local copies, waits for them, and re-layouts: 0.9 us -> 16.8 us
  matrix products: 49.9 us -> 43.4 us
    reshape x0 -> x1, local copies, waits for them, and re-layouts: none -> 10.2 us  [store_the_levels_all(): return jnp.concatenate(all_values, dim_no)]
    unnamed x44 -> x63, local copies, waits for them, and re-layouts: 0.61 us -> 6.3 us
  transfers between devices with their start and end apart: 7 -> 7, of which waited for: 4 -> 4; matrix products, arithmetic and copies ran while one was open for 10% -> 9% of each run, Pallas kernels for 0% -> 0%
where the time goes in v1:
time: 377 us
  waiting for transfers between devices  148 us (39%)
  blocking collectives  137 us (36%)
  matrix products  43.4 us (12%)
  local copies, waits for them, and re-layouts  16.8 us (4%)
  between operations  14.2 us (4%)
  other arithmetic  12.5 us (3%)
  starting transfers between devices  5.25 us (1%)
    reduce_scatter x1, waiting for transfers between devices, on_device(): lax.psum_scatter(expert_term, 'tp', scatter_dimension=2, tiled=True)  58 us
    reduce_scatter x1, waiting for transfers between devices, on_device(): lax.psum_scatter(jnp.einsum('td,tc->dc', grad_resid, merged, preferred_el...  45.7 us
    all_to_all x1, blocking collectives, on_device(): lax.all_to_all(sent_rows, 'sp', split_axis=0, concat_axis=0, tiled=True)  44.2 us
    all_to_all x1, blocking collectives, on_device(): lax.all_to_all(summed, 'sp', split_axis=0, concat_axis=0, tiled=True)  42.3 us
    all_to_all x1, blocking collectives, on_device(): lax.all_to_all(sent_cots, 'sp', split_axis=0, concat_axis=0, tiled=True)  40.2 us
    all_gather x1, waiting for transfers between devices, store_the_levels_all(): all_values = lax.all_gather(slab_in, axis_name='tp')  30.3 us
    all_gather x1, waiting for transfers between devices, on_device(): lax.all_gather(own_grad.astype(bf16), 'tp', axis=1, tiled=True).astype(f32)  14.1 us
    reshape x1, local copies, waits for them, and re-layouts, store_the_levels_all(): return jnp.concatenate(all_values, dim_no)  10.2 us
  transfers between devices with their start and end apart: 7, of which 4 were waited for; matrix products, arithmetic and copies ran while one was open for 9% of the time, Pallas kernels for 0%

profile of v1, /device:TPU:0, one launch (start us, length us, event | category | flops | bytes accessed | tf_op | source)
XLA Modules:
  0.0 376.9 jit_solution(11734461016508358612)
XLA Ops:
  7.2 0.0 all-gather.5.cloned.1.call-start
  7.3 3.6 convert_element_type.75
  10.9 0.4 multiply_reduce_fusion.1
  11.3 0.1 convolution_convert_fusion.3
  11.4 0.1 select_reduce_fusion
  11.5 0.1 dynamic-slice
  11.6 2.2 convolution_convert_fusion.1
  13.8 44.2 %all_to_all.24 = bf16[8,192,512]{2,1,0:T(8,128)(2,1)} all-to-all(bf16[8,192,512]{2,1,0:T(8,128)(2,1)S(1)} %bitcast.58), channel_id=1, replica_groups=mesh['sp'=8,'tp'=4] {'sp'}, dimensions={0} | all-to-all | bytes 3145728 | tf_op jit(solution)/shard_map/all_to_all | solution.py:100
  58.0 0.0 all-gather.5.cloned.1.call-update
  58.1 0.0 all-gather.9.cloned.1.call-start
  58.1 2.0 convolution_convert_fusion
  60.1 40.2 %all_to_all.25 = bf16[8,192,512]{2,1,0:T(8,128)(2,1)} all-to-all(bf16[8,192,512]{2,1,0:T(8,128)(2,1)S(1)} %bitcast.59), channel_id=1, replica_groups=mesh['sp'=8,'tp'=4] {'sp'}, dimensions={0} | all-to-all | bytes 3145728 | tf_op jit(solution)/shard_map/all_to_all | solution.py:106
  100.3 0.0 all-gather.9.cloned.1.call-update
  100.3 0.0 reduce-scatter.3.cloned.1.call-start
  100.4 0.6 add_reduce_fusion
  101.0 0.1 all_to_all.17
  101.1 9.9 %all_to_all.26 = f32[8,1,192]{2,1,0:T(1,128)S(1)} all-to-all(f32[8,1,192]{2,1,0:T(1,128)S(1)} %all_to_all.17), channel_id=1, replica_groups=mesh['sp'=8,'tp'=4] {'sp'}, dimensions={0} | all-to-all | bytes 12288 | tf_op jit(solution)/shard_map/all_to_all | solution.py:98
  110.9 0.1 mul.171
  111.0 6.7 %fusion.17 = f32[1536,256]{1,0:T(8,128)} fusion(bf16[1536,2048]{1,0:T(8,128)(2,1)} %bitcast.66, bf16[1,2048,256]{2,1,0:T(8,128)(2,1)S(1)} %copy-done), kind=kOutput, calls=%fused_computation.32 | convolution fusion | flops 1610612736 | bytes 8912896 | tf_op jit(solution)/shard_map/dot_general | solution.py:18
  117.7 0.5 copy-done.21
  118.2 3.0 fusion.20
  121.2 30.3 %all-gather.9.cloned.1.call-done = bf16[32,192,512]{2,1,0:T(8,128)(2,1)} async-done(((bf16[8,192,512]{2,1,0:T(8,128)(2,1)}), bf16[32,192,512]{2,1,0:T(8,128)(2,1)}) %all-gather.9.cloned.1.call-update) | async-done | bytes 6291472 | tf_op jit(solution)/shard_map/all_gather | solution.py:55
  151.5 10.2 %copy.31 = bf16[8,192,4,512]{3,2,1,0:T(4,128)(2,1)} copy(bf16[8,192,4,512]{3,1,0,2:T(8,128)(2,1)} %bitcast.56) | data formatting | bytes 12582912 | tf_op jit(solution)/shard_map/reshape | solution.py:56
  161.8 5.6 %copy.32 = bf16[192,8,4,512]{3,1,2,0:T(8,128)(2,1)S(1)} copy(bf16[192,8,4,512]{3,2,1,0:T(4,128)(2,1)} %bitcast.50) | data formatting | bytes 12582912
  167.5 2.8 multiply_convert_fusion.1
  170.3 1.8 fusion.15
  172.1 4.4 %add_convert_fusion = bf16[1536,2048]{1,0:T(8,128)(2,1)} fusion(f32[1536,2048]{1,0:T(8,128)S(1)} %fusion.15, bf16[1536,256]{1,0:T(8,128)(2,1)S(1)} %get-tuple-element.16, bf16[1,2048,256]{2,1,0:T(8,128)(2,1)S(1)} %copy-done.9), kind=kOutput, calls=%fused_computation | convolution fusion | flops 1616904192 | bytes 20709376 | tf_op jit(solution)/shard_map/rf,df->rd/dot_general | solution.py:32
  176.6 0.0 all-gather.7.cloned.1.call-start
  176.6 58.0 %reduce-scatter.3.cloned.1.call-done = bf16[8,192,512]{2,1,0:T(8,128)(2,1)} async-done(((bf16[8,192,2048]{2,1,0:T(8,128)(2,1)}), bf16[8,192,512]{2,1,0:T(8,128)(2,1)}) %reduce-scatter.3.cloned.1.call-update) | async-done | bytes 1572880 | tf_op jit(solution)/shard_map/reduce_scatter | solution.py:121
  234.6 42.3 %all_to_all.27 = bf16[8,192,512]{2,1,0:T(8,128)(2,1)S(1)} all-to-all(bf16[8,192,512]{2,1,0:T(8,128)(2,1)} %reduce-scatter.3.cloned.1.call-done), channel_id=1, replica_groups=mesh['sp'=8,'tp'=4] {'sp'}, dimensions={0} | all-to-all | bytes 3145728 | tf_op jit(solution)/shard_map/all_to_all | solution.py:125
  277.0 1.6 fusion.6
  278.5 0.0 all-gather.7.cloned.1.call-update
  278.6 0.0 reduce-scatter.5.cloned.1.call-start
  278.7 3.6 collective-permute-start
  282.4 14.1 %all-gather.7.cloned.1.call-done = bf16[384,2048]{1,0:T(8,128)(2,1)} async-done(((bf16[384,512]{1,0:T(8,128)(2,1)}), bf16[384,2048]{1,0:T(8,128)(2,1)}) %all-gather.7.cloned.1.call-update) | async-done | bytes 1572880 | tf_op jit(solution)/shard_map/all_gather | solution.py:129
  296.4 2.1 multiply_reduce_fusion
  298.6 2.5 subtract_convert_fusion
  301.2 1.4 multiply_convert_fusion.4
  302.6 1.8 convolution_convert_fusion.2
  304.4 0.0 reduce-scatter.5.cloned.1.call-update
  304.5 6.2 %convolution_bitcast_fusion.2 = f32[1,2048,256]{2,1,0:T(8,128)} fusion(bf16[1536,2048]{1,0:T(8,128)(2,1)} %bitcast.67, bf16[1536,256]{1,0:T(8,128)(2,1)S(1)} %copy-done.7), kind=kOutput, calls=%fused_computation.10 | convolution fusion | flops 1610612736 | bytes 9175040 | tf_op jit(solution)/shard_map/rd,rf->df/dot_general | solution.py:30
  310.7 3.3 convolution_bitcast_fusion
  314.0 1.4 collective-permute-start.1
  315.4 6.1 %convolution_bitcast_fusion.1 = f32[1,2048,256]{2,1,0:T(8,128)} fusion(bf16[1536,2048]{1,0:T(8,128)(2,1)} %bitcast.68, bf16[1536,256]{1,0:T(8,128)(2,1)S(1)} %copy-done.11), kind=kOutput, calls=%fused_computation.9 | convolution fusion | flops 1610612736 | bytes 9175040 | tf_op jit(solution)/shard_map/rd,rf->df/dot_general | solution.py:31
  321.5 0.8 fusion.35
  322.4 0.7 fusion.36
  323.1 45.7 %reduce-scatter.5.cloned.1.call-done = bf16[256,256]{1,0:T(8,128)(2,1)} async-done(((bf16[2048,256]{1,0:T(8,128)(2,1)}), bf16[256,256]{1,0:T(8,128)(2,1)}) %reduce-scatter.5.cloned.1.call-update) | async-done | bytes 131088 | tf_op jit(solution)/shard_map/reduce_scatter | solution.py:144
  368.8 1.6 convert_element_type.92
  (77 shorter events, 0.3 us)
Async XLA Ops:
  7.2 103.9 %copy-start = (bf16[1,2048,256]{2,1,0:T(8,128)(2,1)S(1)}, bf16[1,2048,256]{2,1,0:T(8,128)(2,1)}, u32[]{:S(2)}) copy-start(bf16[1,2048,256]{2,1,0:T(8,128)(2,1)} %param.18) | copy-start | bytes 3145732
  7.2 103.8 %all-gather.5.cloned.1.call-start = ((), (), s32[]{:S(2)}) async-start(), calls=%async_computation.6 | async-start | bytes 7864320 | tf_op jit(solution)/shard_map/all_gather | solution.py:99
  7.2 3.6 copy-start.2
  7.2 4.0 %copy-start.16 = (s32[384,2]{0,1:T(2,128)S(1)}, s32[384,2]{0,1:T(2,128)}, u32[]{:S(2)}) copy-start(s32[384,2]{0,1:T(2,128)} %param.16) | copy-start | bytes 9220
  7.3 4.3 %copy-start.15 = (f32[2048]{0:T(1024)S(1)}, f32[2048]{0:T(1024)}, u32[]{:S(2)}) copy-start(f32[2048]{0:T(1024)} %param.15) | copy-start | bytes 24580
  58.1 93.5 %all-gather.9.cloned.1.call-start = ((), (), s32[]{:S(2)}) async-start(), calls=%async_computation.10 | async-start | bytes 7864320 | tf_op jit(solution)/shard_map/all_gather | solution.py:55
  60.1 40.3 %copy-start.19 = (f32[384,2]{0,1:T(2,128)S(1)}, f32[384,2]{0,1:T(2,128)}, u32[]{:S(2)}) copy-start(f32[384,2]{0,1:T(2,128)} %param.17) | copy-start | bytes 9220
  100.3 134.3 %reduce-scatter.3.cloned.1.call-start = ((), (), s32[]{:S(2)}) async-start(), calls=%async_computation.7 | async-start | bytes 7864320 | tf_op jit(solution)/shard_map/reduce_scatter | solution.py:121
  111.0 6.7 %copy-start.8 = (bf16[1,2048,256]{2,1,0:T(8,128)(2,1)S(1)}, bf16[1,2048,256]{2,1,0:T(8,128)(2,1)}, u32[]{:S(2)}) copy-start(bf16[1,2048,256]{2,1,0:T(8,128)(2,1)} %param.19) | copy-start | bytes 3145732
  111.0 7.2 %copy-start.21 = (bf16[8,192,2048]{2,1,0:T(8,128)(2,1)S(1)}, bf16[8,192,2048]{2,1,0:T(8,128)(2,1)}, u32[]{:S(2)}) copy-start(bf16[8,192,2048]{2,1,0:T(8,128)(2,1)} %all-gather.5.cloned.1.call-done) | copy-start | bytes 18874372
  161.8 5.7 %copy-start.22 = (bf16[1,256,2048]{2,1,0:T(8,128)(2,1)S(1)}, bf16[1,256,2048]{2,1,0:T(8,128)(2,1)}, u32[]{:S(2)}) copy-start(bf16[1,256,2048]{2,1,0:T(8,128)(2,1)} %param.20) | copy-start | bytes 3145732
  161.8 5.7 %copy-start.25 = (f32[1536,256]{1,0:T(8,128)S(1)}, f32[1536,256]{1,0:T(8,128)}, u32[]{:S(2)}) copy-start(f32[1536,256]{1,0:T(8,128)} %fusion.17) | copy-start | bytes 4718596
  161.8 5.7 %copy-start.27 = (f32[1536,256]{1,0:T(8,128)S(1)}, f32[1536,256]{1,0:T(8,128)}, u32[]{:S(2)}) copy-start(f32[1536,256]{1,0:T(8,128)} %fusion.20) | copy-start | bytes 4718596
  167.4 2.8 copy-start.3
  170.2 1.9 copy-start.6
  170.2 1.9 copy-start.10
  170.3 1.9 copy-start.9
  176.6 119.8 %all-gather.7.cloned.1.call-start = ((), (), s32[]{:S(2)}) async-start(), calls=%async_computation.8 | async-start | bytes 1966080 | tf_op jit(solution)/shard_map/all_gather | solution.py:129
  277.0 1.7 copy-start.12
  277.0 1.7 copy-start.13
  277.0 5.4 %copy-start.20 = (f32[3,256]{1,0:T(4,128)S(1)}, f32[3,256]{1,0:T(4,128)}, u32[]{:S(2)}) copy-start(f32[3,256]{1,0:T(4,128)} %param.25) | copy-start | bytes 9220
  278.6 90.2 %reduce-scatter.5.cloned.1.call-start = ((), (), s32[]{:S(2)}) async-start(), calls=%async_computation.9 | async-start | bytes 1179648 | tf_op jit(solution)/shard_map/reduce_scatter | solution.py:144
  278.7 22.4 %collective-permute-start = (f32[2,256]{1,0:T(2,128)S(1)}, f32[2,256]{1,0:T(2,128)S(1)}, u32[]{:S(2)}, u32[]{:S(2)}) collective-permute-start(f32[2,256]{1,0:T(2,128)S(1)} %slice.57), channel_id=1, source_target_pairs={{0,4},{4,8},{8,12},{12,16},{16,20},{20,24},{24,28},{1,5},{5,9},{9,... | collective-permute-start | bytes 6152 | tf_op jit(solution)/shard_map/ppermute | solution.py:12
  282.4 18.8 %copy-start.17 = (f32[1,256]{1,0:T(1,128)}, f32[1,256]{1,0:T(1,128)S(1)}, u32[]{:S(2)}) copy-start(f32[1,256]{1,0:T(1,128)S(1)} %get-tuple-element.21) | copy-start | bytes 3076
  296.4 2.1 copy-start.4
  298.6 2.6 copy-start.23
  298.6 2.6 copy-start.24
  301.1 1.5 copy-start.5
  302.6 1.8 copy-start.7
  304.4 6.2 %slice-start = ((s8[6291456]{0:T(1024)(128)(4,1)}), s8[2097152]{0:T(1024)(128)(4,1)S(1)}, s32[]{:S(2)}) async-start(s8[6291456]{0:T(1024)(128)(4,1)} %bitcast.53), calls=%async_computation.11 | async-start | bytes 4194304
  304.4 6.2 %slice-start.1 = ((s8[6291456]{0:T(1024)(128)(4,1)}), s8[4194304]{0:T(1024)(128)(4,1)S(1)}, s32[]{:S(2)}) async-start(s8[6291456]{0:T(1024)(128)(4,1)} %bitcast.53), calls=%async_computation.12 | async-start | bytes 8388608
  304.4 6.2 %copy-start.26 = (f32[1536,256]{1,0:T(8,128)S(1)}, f32[1536,256]{1,0:T(8,128)}, u32[]{:S(2)}) copy-start(f32[1536,256]{1,0:T(8,128)} %fusion.17) | copy-start | bytes 4718596
  304.4 6.2 %copy-start.28 = (f32[1536,256]{1,0:T(8,128)S(1)}, f32[1536,256]{1,0:T(8,128)}, u32[]{:S(2)}) copy-start(f32[1536,256]{1,0:T(8,128)} %fusion.20) | copy-start | bytes 4718596
  310.7 3.3 copy-start.14
  310.7 4.7 %copy-start.11 = (bf16[1536,256]{1,0:T(8,128)(2,1)S(1)}, bf16[1536,256]{1,0:T(8,128)(2,1)}, u32[]{:S(2)}) copy-start(bf16[1536,256]{1,0:T(8,128)(2,1)} %copy-done.10) | copy-start | bytes 2359300
  314.0 7.6 %copy-start.18 = (f32[1,256]{1,0:T(1,128)S(1)}, f32[1,256]{1,0:T(1,128)}, u32[]{:S(2)}) copy-start(f32[1,256]{1,0:T(1,128)} %copy-done.17) | copy-start | bytes 3076
  314.0 7.6 %collective-permute-start.1 = (f32[2,256]{1,0:T(2,128)S(1)}, f32[2,256]{1,0:T(2,128)S(1)}, u32[]{:S(2)}, u32[]{:S(2)}) collective-permute-start(f32[2,256]{1,0:T(2,128)S(1)} %slice.60), channel_id=1, source_target_pairs={{4,0},{8,4},{12,8},{16,12},{20,16},{24,20},{28,24},{5,1},{9,5},{13... | collective-permute-start | bytes 6152 | tf_op jit(solution)/shard_map/ppermute | solution.py:12
  315.4 55.0 %copy-start.1 = (bf16[1,2048,256]{2,1,0:T(8,128)(2,1)S(1)}, bf16[1,2048,256]{2,1,0:T(8,128)(2,1)}, u32[]{:S(2)}) copy-start(bf16[1,2048,256]{2,1,0:T(8,128)(2,1)} %param.18) | copy-start | bytes 3145732
Sparse Core Ops, SparseCore 0:
  58.2 45.3 all-gather.4
  105.1 46.3 all-gather.8
  176.7 57.8 reduce-scatter.2
  278.7 17.7 all-gather.6
  304.5 64.1 reduce-scatter.4
